TPU v7x, 256 devices: a whole 4x4x8 slice. The times are simulated.
256 devices in a mesh: sp: 64 (over z, x, core), tp: 4 (over y).
Axes of the slice: x: 4, y: 4, z: 8, core: 2. Of those that a mesh axis runs over, the one named last changes fastest.
Arguments:
- residual: bfloat16 [24576, 2048], P(('sp', 'tp')), may hold values from -6 to 6
- queries: bfloat16 [24576, 1024], P('sp', 'tp'), may hold values from -2.5 to 2.5
- keys: bfloat16 [24576, 256], P('sp', 'tp'), may hold values from -2.5 to 2.5
- values: bfloat16 [24576, 256], P('sp', 'tp'), may hold values from -6 to 6
- documents: int32 [24576], P('sp'), may hold values from 0 to 32, never falling along the last dimension, each value on 1 to 1536 neighbouring positions
- sink: float32 [16], P('tp'), may hold values from 3 to 7
- out_weight: bfloat16 [1024, 2048], replicated, may hold values from -0.1875 to 0.1875
- mix_gain: float32 [2048], replicated, may hold values from 0.1 to 1.9
- ffn_gain: float32 [2048], replicated, may hold values from 0.1 to 1.9
- out_gain: float32 [2048], replicated, may hold values from 0.1 to 1.9
- routes: int32 [24576, 4], P(('sp', 'tp')), may hold values from 0 to 63, all different within a row; in each aligned block of 96 rows (0 to 95, 96 to 191, ...) at most 8 rows name the same one
- route_logits: float32 [24576, 4], P(('sp', 'tp')), may hold values from -4 to 4
- gate_weight: bfloat16 [64, 2048, 2048], P('sp', None, 'tp'), may hold values from -1.41421356 to 1.41421356
- up_weight: bfloat16 [64, 2048, 2048], P('sp', None, 'tp'), may hold values from -1.41421356 to 1.41421356
- down_weight: bfloat16 [64, 2048, 2048], P('sp', 'tp'), may hold values from -0.125 to 0.125
Outputs:
- mixed: bfloat16 [24576, 2048], P(('sp', 'tp'))
Inputs may be any that keep to these rules, and one draw needn't show every extreme that they name: `routes`: each row names 4 different experts. In each aligned block of rows held by one device, no expert is named by more than 8 rows, a bound that some block reaches. `documents`: document numbers never fall along the positions; each document has 1 to 1536 positions, and one has exactly 1536.
All inputs are finite; a program needn't handle non-finite values.
Results may differ from a plain program's by a relative error of at most 0.017.
Values may be sent and summed in bfloat16 or wider, within the bound.
A program may use at most 128 MiB of HBM per device.

v0:
```python
import jax
import jax.numpy as jnp
from jax import lax
from jax.sharding import PartitionSpec as P

HD = 64
TOPK = 4
W = 128


def extended(block, sides, width):
    for axis, dim in sides:
        count = lax.axis_size(axis)
        forward = [(i, i + 1) for i in range(count - 1)]
        backward = [(target, source) for source, target in forward]
        low = lax.ppermute(
            lax.slice_in_dim(block, block.shape[dim] - width, None, axis=dim), axis, forward
        )
        high = lax.ppermute(lax.slice_in_dim(block, 0, width, axis=dim), axis, backward)
        block = jnp.concatenate([low, block, high], axis=dim)
    return block


def turn_heads(block, positions, head_count):
    total = block.shape[0]
    heads = block.astype(jnp.float32).reshape(total, head_count, HD)
    half_size = HD // 2
    inverse = 10000.0 ** (-jnp.arange(half_size, dtype=jnp.float32) / half_size)
    angles = positions.astype(jnp.float32)[:, None] * inverse[None, :]
    cosine = jnp.cos(angles)[:, None, :]
    sine = jnp.sin(angles)[:, None, :]
    first_half = heads[..., :half_size]
    second_half = heads[..., half_size:]
    turned = jnp.concatenate(
        [first_half * cosine - second_half * sine, second_half * cosine + first_half * sine],
        axis=-1,
    )
    return turned.reshape(total, head_count * HD).astype(jnp.bfloat16)


def rms_scale(vector):
    return vector * lax.rsqrt(jnp.mean(vector * vector, axis=-1, keepdims=True) + 1e-06)


def windows(padded_rows, blocks):
    tiled = padded_rows.reshape((blocks + 2, W) + padded_rows.shape[1:])
    return jnp.concatenate([tiled[:-2], tiled[1:-1], tiled[2:]], axis=1)


def assign_slots(route_rows, expert_count, capacity):
    flat_routes = route_rows.reshape(route_rows.shape[0] * TOPK)
    onehot_hits = (
        flat_routes[:, None] == jnp.arange(expert_count, dtype=jnp.int32)[None, :]
    ).astype(jnp.int32)
    slot_number = jnp.sum(jnp.cumsum(onehot_hits, axis=0) * onehot_hits, axis=1) - 1
    return flat_routes * capacity + slot_number


def body(
    residual,
    queries,
    keys,
    values,
    documents,
    sink,
    out_weight,
    mix_gain,
    ffn_gain,
    out_gain,
    routes,
    route_logits,
    gate_weight,
    up_weight,
    down_weight,
):
    tok_rows = queries.shape[0]
    head_count = queries.shape[1] // HD
    kv_count = keys.shape[1] // HD
    group_size = head_count // kv_count
    sp_count = lax.axis_size("sp")
    tp_count = lax.axis_size("tp")
    offset = lax.axis_index("sp") * tok_rows
    positions = offset + jnp.arange(tok_rows, dtype=jnp.int32)
    q_turned = turn_heads(queries, positions, head_count)
    k_turned = turn_heads(keys, positions, kv_count)
    paired = jnp.concatenate([k_turned, values], axis=1)
    wide_pairs, wide_docs = (
        extended(paired, (("sp", 0),), W),
        extended(documents, (("sp", 0),), W),
    )
    blocks = tok_rows // W
    query_blocks = q_turned.reshape(blocks, W, kv_count, group_size, HD)
    pair_win = windows(wide_pairs, blocks)
    key_win = pair_win[..., : kv_count * HD].reshape(blocks, 3 * W, kv_count, HD)
    value_win = pair_win[..., kv_count * HD :].reshape(blocks, 3 * W, kv_count, HD)
    doc_win = windows(wide_docs, blocks)
    doc_query = documents.reshape(blocks, W)
    block_ids = jnp.arange(blocks, dtype=jnp.int32)[:, None, None]
    query_pos = offset + block_ids * W + jnp.arange(W, dtype=jnp.int32)[None, :, None]
    key_pos = offset + (block_ids - 1) * W + jnp.arange(3 * W, dtype=jnp.int32)[None, None, :]
    keep_mask = (
        (jnp.abs(query_pos - key_pos) <= W) & (key_pos >= 0) & (key_pos < tok_rows * sp_count)
    )
    keep_mask = keep_mask & (doc_query[:, :, None] == doc_win[:, None, :])
    scores = jnp.einsum(
        "nqhgd,nkhd->nhgqk", query_blocks, key_win, preferred_element_type=jnp.float32
    ) * HD ** (-0.5)
    exponent = jnp.where(keep_mask[:, None, None], jnp.exp(scores), 0.0)
    denominator = jnp.sum(exponent, axis=-1, keepdims=True) + jnp.exp(sink).reshape(
        1, kv_count, group_size, 1, 1
    )
    probs = (exponent / denominator).astype(jnp.bfloat16)
    attended = jnp.einsum("nhgqk,nkhd->nqhgd", probs, value_win, preferred_element_type=jnp.float32)
    attended = attended.astype(jnp.bfloat16).reshape(tok_rows, head_count * HD)
    own_rows = tok_rows // tp_count
    all_heads = lax.all_to_all(attended, "tp", split_axis=0, concat_axis=1, tiled=True)
    projected = jnp.dot(all_heads, out_weight, preferred_element_type=jnp.float32)
    after_mix = residual.astype(jnp.float32) + rms_scale(projected) * mix_gain
    normed = (rms_scale(after_mix) * ffn_gain).astype(jnp.bfloat16)
    local_experts = gate_weight.shape[0]
    expert_count = local_experts * sp_count
    capacity = max(2, own_rows * TOPK * 4 // (3 * expert_count))
    slot_index = assign_slots(routes, expert_count, capacity)
    token_of = jnp.arange(own_rows * TOPK, dtype=jnp.int32) // TOPK
    model_width = normed.shape[1]
    filled = jnp.full((expert_count * capacity,), own_rows, jnp.int32).at[slot_index].set(token_of)
    with_zero = jnp.concatenate([normed, jnp.zeros((1, model_width), jnp.bfloat16)], axis=0)
    outgoing = with_zero[filled].reshape(expert_count, capacity, model_width)
    incoming = lax.all_to_all(outgoing, "sp", split_axis=0, concat_axis=1, tiled=True)
    rows_in = lax.all_gather(incoming, "tp", axis=1, tiled=True)
    gate_pre = jnp.einsum("erd,edf->erf", rows_in, gate_weight, preferred_element_type=jnp.float32)
    up_pre = jnp.einsum("erd,edf->erf", rows_in, up_weight, preferred_element_type=jnp.float32)
    gated = jnp.minimum(gate_pre, 7.0)
    upper = jnp.clip(up_pre, -7.0, 7.0)
    hidden = ((upper + 1.0) * gated * jax.nn.sigmoid(1.702 * gated)).astype(jnp.bfloat16)
    terms = jnp.einsum("erf,efd->erd", hidden, down_weight, preferred_element_type=jnp.float32)
    own_terms = lax.psum_scatter(terms.astype(jnp.bfloat16), "tp", scatter_dimension=1, tiled=True)
    returned = lax.all_to_all(own_terms, "sp", split_axis=1, concat_axis=0, tiled=True)
    picked = returned.reshape(expert_count * capacity, model_width)[slot_index]
    picked = picked.reshape(own_rows, TOPK, model_width).astype(jnp.float32)
    exp_logits = jnp.exp(route_logits)
    route_weights = exp_logits / jnp.sum(exp_logits, axis=-1, keepdims=True)
    expert_mix = jnp.einsum("rk,rkd->rd", route_weights, picked)
    return (after_mix + rms_scale(expert_mix) * out_gain).astype(jnp.bfloat16)


def solution(mesh):
    in_specs = (
        P(("sp", "tp"), None),
        P("sp", "tp"),
        P("sp", "tp"),
        P("sp", "tp"),
        P("sp"),
        P("tp"),
        P(),
        P(),
        P(),
        P(),
        P(("sp", "tp"), None),
        P(("sp", "tp"), None),
        P("sp", None, "tp"),
        P("sp", None, "tp"),
        P("sp", "tp", None),
    )
    out_specs = P(("sp", "tp"), None)
    return jax.shard_map(body, mesh=mesh, in_specs=in_specs, out_specs=out_specs, check_vma=False)
```

profile of v0, /device:TPU:2, one launch (start us, length us, event | category | flops | bytes accessed | tf_op | source)
XLA Modules:
  0.0 421.9 jit_solution(6266095568807970665)
XLA Ops:
  6.6 1.0 bitcast_convert_fusion
  7.5 0.3 fusion.44
  7.8 0.7 fusion.47
  8.6 1.9 collective-permute-start
  10.5 3.6 collective-permute-start.1
  14.1 0.8 fusion.63
  14.9 1.9 collective-permute-start.2
  16.8 3.6 collective-permute-start.3
  20.5 0.1 fusion.50
  20.5 0.1 iota_add_fusion
  20.6 0.3 multiply_cosine_fusion
  20.9 0.8 copy.76
  21.6 0.1 eq.52
  21.8 0.1 eq.48
  21.9 0.7 broadcast_multiply_fusion
  22.6 0.1 iota_add_fusion.1
  22.6 1.1 copy.69
  23.8 0.9 reduce-window.6
  24.7 0.2 slice_reduce_fusion
  24.9 0.1 fusion.37
  25.1 0.1 copy.75
  25.2 0.1 mul.230
  25.3 0.1 subtract_convert_fusion
  25.4 2.9 scatter_custom_fusion
  28.4 0.9 fusion.32
  29.3 0.1 copy.63
  29.5 0.1 copy.66
  29.6 0.1 copy.64
  29.7 0.1 copy.67
  29.9 0.1 copy.65
  30.0 0.1 copy.68
  30.2 0.7 fusion.17
  30.9 0.1 broadcast_add_fusion
  30.9 0.7 fusion.23
  31.6 0.3 copy.85
  31.9 1.0 reshape.463
  32.8 4.5 %all-to-all-start = ((bf16[4,96,256]{2,1,0:T(8,128)(2,1)}), bf16[4,96,256]{2,1,0:T(8,128)(2,1)S(1)}, u32[]{:S(2)}, u32[]{:S(2)}) async-start(bf16[4,96,256]{2,1,0:T(8,128)(2,1)} %reshape.463), calls=%async_computation | async-start | bytes 393216 | tf_op jit(solution)/shard_map/all_to_all | solution.py:116
  37.3 6.3 %all-to-all-done = bf16[4,96,256]{2,1,0:T(8,128)(2,1)S(1)} async-done(((bf16[4,96,256]{2,1,0:T(8,128)(2,1)}), bf16[4,96,256]{2,1,0:T(8,128)(2,1)S(1)}, u32[]{:S(2)}, u32[]{:S(2)}) %all-to-all-start) | async-done | bytes 196640 | tf_op jit(solution)/shard_map/all_to_all | solution.py:116
  43.7 3.1 multiply_reduce_fusion.1
  46.8 0.3 multiply_reduce_fusion
  47.2 0.3 multiply_convert_fusion.1
  47.5 3.3 gather_fusion
  50.8 67.5 %all_to_all.40 = bf16[64,8,2048]{2,1,0:T(8,128)(2,1)} all-to-all(bf16[64,8,2048]{2,1,0:T(8,128)(2,1)} %bitcast.134), channel_id=1, replica_groups=mesh['sp'=64,'tp'=4] {'sp'}, dimensions={0} | all-to-all | bytes 4194304 | tf_op jit(solution)/shard_map/all_to_all | solution.py:129
  118.4 0.0 all-gather.2.cloned.1.call-update
  118.4 0.2 reduce-scatter.2.cloned.1.call-start
  118.6 79.9 %all-gather.2.cloned.1.call-done = bf16[1,2048,2048]{2,1,0:T(8,128)(2,1)} async-done(((bf16[1,512,2048]{2,1,0:T(8,128)(2,1)}), bf16[1,2048,2048]{2,1,0:T(8,128)(2,1)}) %all-gather.2.cloned.1.call-update) | async-done | bytes 8388624 | tf_op jit(solution)/shard_map/all_gather | solution.py:130
  198.5 10.4 %fusion = f32[2048,512]{1,0:T(8,128)} fusion(bf16[1,2048,2048]{2,1,0:T(8,128)(2,1)} %all-gather.2.cloned.1.call-done, bf16[1,2048,512]{2,1,0:T(8,128)(2,1)} %param.27), kind=kOutput, calls=%fused_computation.3 | convolution fusion | flops 4294967296 | bytes 14680064 | tf_op jit(solution)/shard_map/erd,edf->erf/dot_general | solution.py:131
  209.0 15.2 %convert_bitcast_fusion = bf16[1,2048,2048]{2,1,0:T(8,128)(2,1)} fusion(bf16[1,512,2048]{2,1,0:T(8,128)(2,1)S(1)} %copy-done, f32[2048,512]{1,0:T(8,128)} %fusion, bf16[1,2048,2048]{2,1,0:T(8,128)(2,1)} %all-gather.2.cloned.1.call-done, bf16[1,2048,512]{2,1,0:T(8,128)(2,1)} %param.28), kind=kOutput, calls=%fused_computation.7 | convolution fusion | flops 8604614656 | bytes 25165824 | tf_op jit(solution)/shard_map/erf,efd->erd/dot_general | solution.py:136
  224.1 0.0 reduce-scatter.2.cloned.1.call-update
  224.2 84.2 %reduce-scatter.2.cloned.1.call-done = bf16[1,512,2048]{2,1,0:T(8,128)(2,1)} async-done(((bf16[1,2048,2048]{2,1,0:T(8,128)(2,1)}), bf16[1,512,2048]{2,1,0:T(8,128)(2,1)}) %reduce-scatter.2.cloned.1.call-update) | async-done | bytes 2097168 | tf_op jit(solution)/shard_map/reduce_scatter | solution.py:137
  308.4 6.7 %copy.103 = bf16[1,512,2048]{2,0,1:T(2,128)(2,1)} copy(bf16[1,512,2048]{2,1,0:T(8,128)(2,1)} %reduce-scatter.2.cloned.1.call-done) | data formatting | bytes 4194304 | tf_op jit(solution)/shard_map/reduce_scatter | solution.py:137
  315.1 0.5 broadcast.380
  315.6 13.2 %reduce.5 = bf16[512,2048]{1,0:T(8,128)(2,1)S(1)} reduce(bf16[512,1,2048]{2,1,0:T(2,128)(2,1)} %bitcast.132, bf16[]{:T(256)} %broadcast.380), dimensions={1}, to_apply=%bitcast.129.reduce_sub_computation | reduce | bytes 4194306
  328.8 3.3 reshape.468
  332.1 10.7 %all-to-all-start.2 = ((bf16[64,2,8192]{2,1,0:T(2,128)(2,1)}), bf16[64,2,8192]{2,1,0:T(2,128)(2,1)S(1)}, u32[]{:S(2)}, u32[]{:S(2)}) async-start(bf16[64,2,8192]{2,1,0:T(2,128)(2,1)} %reshape.468), calls=%async_computation.3 | async-start | bytes 4194304 | tf_op jit(solution)/shard_map/all_to_all | solution.py:138
  342.8 0.1 copy.83
  343.0 51.0 %all-to-all-done.2 = bf16[64,2,8192]{2,1,0:T(2,128)(2,1)S(1)} async-done(((bf16[64,2,8192]{2,1,0:T(2,128)(2,1)}), bf16[64,2,8192]{2,1,0:T(2,128)(2,1)S(1)}, u32[]{:S(2)}, u32[]{:S(2)}) %all-to-all-start.2) | async-done | bytes 2097184 | tf_op jit(solution)/shard_map/all_to_all | solution.py:138
  394.0 6.8 %reshape.469 = bf16[512,1,2048]{2,1,0:T(2,128)(2,1)} reshape(bf16[64,2,8192]{2,1,0:T(2,128)(2,1)S(1)} %all-to-all-done.2) | data formatting | bytes 4194304
  400.8 3.5 copy.102
  404.2 3.1 gather_fusion.1
  407.4 3.6 reshape.429
  411.0 2.5 fusion.64
  413.5 0.3 fusion.26
  413.9 1.2 fusion.29
  (53 shorter events, 0.4 us)
Async XLA Ops:
  6.5 202.4 %copy-start = (bf16[1,512,2048]{2,1,0:T(8,128)(2,1)S(1)}, bf16[1,512,2048]{2,1,0:T(8,128)(2,1)}, u32[]{:S(2)}) copy-start(bf16[1,512,2048]{2,1,0:T(8,128)(2,1)} %param.29) | copy-start | bytes 6291460
  6.5 22.7 %copy-start.4 = (bf16[384,64]{0,1:T(8,128)(2,1)S(1)}, bf16[384,64]{0,1:T(8,128)(2,1)}, u32[]{:S(2)}) copy-start(bf16[384,64]{0,1:T(8,128)(2,1)} %param.18) | copy-start | bytes 147460
  6.5 21.8 %copy-start.6 = (s32[384]{0:T(512)S(1)}, s32[384]{0:T(512)}, u32[]{:S(2)}) copy-start(s32[384]{0:T(512)} %param.19) | copy-start | bytes 4612
  6.5 18.8 %copy-start.10 = (f32[4]{0:T(128)S(1)}, f32[4]{0:T(128)}, u32[]{:S(2)}) copy-start(f32[4]{0:T(128)} %param.20) | copy-start | bytes 52
  8.6 20.7 %collective-permute-start = (bf16[128,128]{0,1:T(8,128)(2,1)S(1)}, bf16[128,128]{0,1:T(8,128)(2,1)S(1)}, u32[]{:S(2)}, u32[]{:S(2)}) collective-permute-start(bf16[128,128]{0,1:T(8,128)(2,1)S(1)} %get-tuple-element.12), channel_id=1, source_target_pairs={{0,4},{4,8},{8,12},{12,16},{16,20},{20,24},{24,28},{28,32},{32,36}... | collective-permute-start | bytes 98312 | tf_op jit(solution)/shard_map/ppermute | solution.py:16
  10.5 18.8 %collective-permute-start.1 = (bf16[128,128]{0,1:T(8,128)(2,1)S(1)}, bf16[128,128]{0,1:T(8,128)(2,1)S(1)}, u32[]{:S(2)}, u32[]{:S(2)}) collective-permute-start(bf16[128,128]{0,1:T(8,128)(2,1)S(1)} %get-tuple-element.13), channel_id=1, source_target_pairs={{4,0},{8,4},{12,8},{16,12},{20,16},{24,20},{28,24},{32,28},{36,32}... | collective-permute-start | bytes 98312 | tf_op jit(solution)/shard_map/ppermute | solution.py:19
  14.9 13.4 %collective-permute-start.2 = (s32[128]{0:T(128)S(1)}, s32[128]{0:T(128)S(1)}, u32[]{:S(2)}, u32[]{:S(2)}) collective-permute-start(s32[128]{0:T(128)S(1)} %get-tuple-element.18), channel_id=1, source_target_pairs={{0,4},{4,8},{8,12},{12,16},{16,20},{20,24},{24,28},{28,32},{32,36}... | collective-permute-start | bytes 1544 | tf_op jit(solution)/shard_map/ppermute | solution.py:16
  16.8 11.5 %collective-permute-start.3 = (s32[128]{0:T(128)S(1)}, s32[128]{0:T(128)S(1)}, u32[]{:S(2)}, u32[]{:S(2)}) collective-permute-start(s32[128]{0:T(128)S(1)} %get-tuple-element.19), channel_id=1, source_target_pairs={{4,0},{8,4},{12,8},{16,12},{20,16},{24,20},{28,24},{32,28},{36,32}... | collective-permute-start | bytes 1544 | tf_op jit(solution)/shard_map/ppermute | solution.py:19
  32.8 10.8 %all-to-all-start = ((bf16[4,96,256]{2,1,0:T(8,128)(2,1)}), bf16[4,96,256]{2,1,0:T(8,128)(2,1)S(1)}, u32[]{:S(2)}, u32[]{:S(2)}) async-start(bf16[4,96,256]{2,1,0:T(8,128)(2,1)} %reshape.463), calls=%async_computation | async-start | bytes 393216 | tf_op jit(solution)/shard_map/all_to_all | solution.py:116
  37.3 161.2 %all-gather.2.cloned.1.call-start = ((), (), s32[]{:S(2)}) async-start(), calls=%async_computation.4 | async-start | bytes 10485760 | tf_op jit(solution)/shard_map/all_gather | solution.py:130
  43.6 3.2 copy-start.2
  43.6 3.2 copy-start.5
  43.7 3.5 copy-start.7
  118.4 190.0 %reduce-scatter.2.cloned.1.call-start = ((), (), s32[]{:S(2)}) async-start(), calls=%async_computation.5 | async-start | bytes 10485760 | tf_op jit(solution)/shard_map/reduce_scatter | solution.py:137
  332.1 10.7 %copy-start.9 = (f32[96,4]{0,1:T(4,128)S(1)}, f32[96,4]{0,1:T(4,128)}, u32[]{:S(2)}) copy-start(f32[96,4]{0,1:T(4,128)} %param.26) | copy-start | bytes 4612
  332.1 61.9 %all-to-all-start.2 = ((bf16[64,2,8192]{2,1,0:T(2,128)(2,1)}), bf16[64,2,8192]{2,1,0:T(2,128)(2,1)S(1)}, u32[]{:S(2)}, u32[]{:S(2)}) async-start(bf16[64,2,8192]{2,1,0:T(2,128)(2,1)} %reshape.468), calls=%async_computation.3 | async-start | bytes 4194304 | tf_op jit(solution)/shard_map/all_to_all | solution.py:138
  411.0 2.8 copy-start.3
  411.0 2.8 copy-start.8
  411.0 4.1 copy-start.1
Sparse Core Ops, SparseCore 0:
  118.5 79.9 all-gather.1
  224.3 84.0 reduce-scatter.1
where the time goes:
time: 423 us; the launch traced here: 422 us
  waiting for transfers between devices  221 us (52%)
  blocking collectives  67.5 us (16%)
  local copies, waits for them, and re-layouts  39.3 us (9%)
  matrix products  32.6 us (8%)
  starting transfers between devices  26.5 us (6%)
  other arithmetic  20.7 us (5%)
  between operations  13.8 us (3%)
    reduce_scatter x1, waiting for transfers between devices, body(): lax.psum_scatter(terms.astype(jnp.bfloat16), 'tp', scatter_dimension=1, t...  84.2 us
    all_gather x1, waiting for transfers between devices, body(): rows_in = lax.all_gather(incoming, 'tp', axis=1, tiled=True)  79.9 us
    all_to_all x1, blocking collectives, body(): lax.all_to_all(outgoing, 'sp', split_axis=0, concat_axis=1, tiled=True)  67.5 us
    all_to_all x1, waiting for transfers between devices, body(): lax.all_to_all(own_terms, 'sp', split_axis=1, concat_axis=0, tiled=True)  51 us
    unnamed x28, local copies, waits for them, and re-layouts  15.9 us
    dot_general x1, matrix products, body(): jnp.einsum('erf,efd->erd', hidden, down_weight, preferred_element_type=jn...  15.2 us
    unnamed x1, other arithmetic  13.2 us
    all_to_all x1, starting transfers between devices, body(): lax.all_to_all(own_terms, 'sp', split_axis=1, concat_axis=0, tiled=True)  10.7 us
  transfers between devices with their start and end apart: 8, of which 4 were waited for; matrix products, arithmetic and copies ran while one was open for 2% of the time, Pallas kernels for 0%

commit v1 on v0

--- a/solution.py
+++ b/solution.py
@@ -1,3 +1,4 @@
+import functools
 import jax
 import jax.numpy as jnp
 from jax import lax
@@ -6,6 +7,14 @@
 HD = 64
 TOPK = 4
 W = 128
+
+
+def terms_map(inputs, mesh_ax):
+    outer = lax.all_to_all(jnp.stack([inputs] * lax.psum(1, mesh_ax)), mesh_ax, 0, 0)
+    return jnp.concatenate(outer, axis=1)
+
+
+indices_meet = functools.partial(terms_map, mesh_ax="tp")
 
 
 def extended(block, sides, width):
@@ -127,7 +136,7 @@
     with_zero = jnp.concatenate([normed, jnp.zeros((1, model_width), jnp.bfloat16)], axis=0)
     outgoing = with_zero[filled].reshape(expert_count, capacity, model_width)
     incoming = lax.all_to_all(outgoing, "sp", split_axis=0, concat_axis=1, tiled=True)
-    rows_in = lax.all_gather(incoming, "tp", axis=1, tiled=True)
+    rows_in = indices_meet(incoming)
     gate_pre = jnp.einsum("erd,edf->erf", rows_in, gate_weight, preferred_element_type=jnp.float32)
     up_pre = jnp.einsum("erd,edf->erf", rows_in, up_weight, preferred_element_type=jnp.float32)
     gated = jnp.minimum(gate_pre, 7.0)

time: 423 us -> 437 us (1.033)
  blocking collectives: 67.5 us -> 163 us
  waiting for transfers between devices: 221 us -> 136 us
  local copies, waits for them, and re-layouts: 39.3 us -> 50.7 us
  matrix products: 32.6 us -> 23.9 us
    all_to_all x0 -> x1, blocking collectives: none -> 95.4 us  [terms_map(): lax.all_to_all(jnp.stack([inputs] * lax.psum(1, mesh_ax)), mesh_ax, 0, 0)]
    all_gather x1 -> x0, waiting for transfers between devices: 79.9 us -> none  [body(): rows_in = lax.all_gather(incoming, 'tp', axis=1, tiled=True)]
    dot_general x1, matrix products: 15.2 us -> 6.79 us  [body(): jnp.einsum('erf,efd->erd', hidden, down_weight, preferred_element_type=jn...]
    unnamed x28 -> x30, local copies, waits for them, and re-layouts: 15.9 us -> 22.5 us
    reduce_scatter x1, waiting for transfers between devices: 84.2 us -> 79 us  [body(): lax.psum_scatter(terms.astype(jnp.bfloat16), 'tp', scatter_dimension=1, t...]
    dot_general x1, matrix products: 10.4 us -> 5.72 us  [body(): jnp.einsum('erd,edf->erf', rows_in, gate_weight, preferred_element_type=j...]
    dot_general x0 -> x1, matrix products: none -> 4.52 us  [body(): jnp.einsum('erd,edf->erf', rows_in, up_weight, preferred_element_type=jnp...]
  transfers between devices with their start and end apart: 8 -> 7, of which waited for: 4 -> 3; matrix products, arithmetic and copies ran while one was open for 2% -> 2% of each run, Pallas kernels for 0% -> 0%
where the time goes in v1:
time: 437 us; the launch traced here: 436 us
  blocking collectives  163 us (37%)
  waiting for transfers between devices  136 us (31%)
  local copies, waits for them, and re-layouts  50.7 us (12%)
  starting transfers between devices  26.4 us (6%)
  matrix products  23.9 us (5%)
  other arithmetic  22.2 us (5%)
  between operations  13.9 us (3%)
    all_to_all x1, blocking collectives, terms_map(): lax.all_to_all(jnp.stack([inputs] * lax.psum(1, mesh_ax)), mesh_ax, 0, 0)  95.4 us
    reduce_scatter x1, waiting for transfers between devices, body(): lax.psum_scatter(terms.astype(jnp.bfloat16), 'tp', scatter_dimension=1, t...  79 us
    all_to_all x1, blocking collectives, body(): lax.all_to_all(outgoing, 'sp', split_axis=0, concat_axis=1, tiled=True)  67.4 us
    all_to_all x1, waiting for transfers between devices, body(): lax.all_to_all(own_terms, 'sp', split_axis=1, concat_axis=0, tiled=True)  51 us
    unnamed x30, local copies, waits for them, and re-layouts  22.5 us
    unnamed x1, other arithmetic  14.7 us
    all_to_all x1, starting transfers between devices, body(): lax.all_to_all(own_terms, 'sp', split_axis=1, concat_axis=0, tiled=True)  10.9 us
  transfers between devices with their start and end apart: 7, of which 3 were waited for; matrix products, arithmetic and copies ran while one was open for 2% of the time, Pallas kernels for 0%

profile of v1, /device:TPU:2, one launch (start us, length us, event | category | flops | bytes accessed | tf_op | source)
XLA Modules:
  0.0 436.3 jit_solution(11198510243865292938)
XLA Ops:
  6.6 1.0 bitcast_convert_fusion
  7.5 0.3 fusion.31
  7.8 0.7 fusion.34
  8.6 1.9 collective-permute-start
  10.5 3.6 collective-permute-start.1
  14.1 0.8 fusion.46
  14.9 1.9 collective-permute-start.2
  16.8 3.6 collective-permute-start.3
  20.5 0.1 fusion.37
  20.5 0.1 iota_add_fusion
  20.6 0.3 multiply_cosine_fusion
  20.9 0.8 copy.76
  21.6 0.1 eq.52
  21.8 0.1 eq.48
  21.9 0.7 broadcast_multiply_fusion
  22.6 0.1 iota_add_fusion.1
  22.6 1.1 copy.69
  23.8 0.9 reduce-window.6
  24.7 0.2 slice_reduce_fusion
  24.9 0.1 fusion.24
  25.1 0.1 copy.75
  25.2 0.1 mul.230
  25.3 0.1 subtract_convert_fusion
  25.4 2.9 scatter_custom_fusion
  28.4 0.9 fusion.19
  29.3 0.1 copy.63
  29.5 0.1 copy.66
  29.6 0.1 copy.64
  29.7 0.1 copy.67
  29.9 0.1 copy.65
  30.0 0.1 copy.68
  30.2 0.7 fusion.4
  30.9 0.1 broadcast_add_fusion
  30.9 0.7 fusion.10
  31.6 0.3 copy.85
  31.9 1.0 reshape.471
  32.8 4.5 %all-to-all-start = ((bf16[4,96,256]{2,1,0:T(8,128)(2,1)}), bf16[4,96,256]{2,1,0:T(8,128)(2,1)S(1)}, u32[]{:S(2)}, u32[]{:S(2)}) async-start(bf16[4,96,256]{2,1,0:T(8,128)(2,1)} %reshape.471), calls=%async_computation | async-start | bytes 393216 | tf_op jit(solution)/shard_map/all_to_all | solution.py:125
  37.3 6.3 %all-to-all-done = bf16[4,96,256]{2,1,0:T(8,128)(2,1)S(1)} async-done(((bf16[4,96,256]{2,1,0:T(8,128)(2,1)}), bf16[4,96,256]{2,1,0:T(8,128)(2,1)S(1)}, u32[]{:S(2)}, u32[]{:S(2)}) %all-to-all-start) | async-done | bytes 196640 | tf_op jit(solution)/shard_map/all_to_all | solution.py:125
  43.7 3.1 multiply_reduce_fusion.1
  46.8 0.3 multiply_reduce_fusion
  47.2 0.3 multiply_convert_fusion.1
  47.5 3.3 gather_fusion
  50.8 67.4 %all_to_all.42 = bf16[64,8,2048]{2,1,0:T(8,128)(2,1)S(1)} all-to-all(bf16[64,8,2048]{2,1,0:T(8,128)(2,1)} %bitcast.127), channel_id=1, replica_groups=mesh['sp'=64,'tp'=4] {'sp'}, dimensions={0} | all-to-all | bytes 4194304 | tf_op jit(solution)/shard_map/all_to_all | solution.py:138
  118.3 1.1 stack.10
  119.4 95.4 %all_to_all.43 = bf16[4,1,512,2048]{3,2,1,0:T(8,128)(2,1)S(1)} all-to-all(bf16[4,1,512,2048]{3,2,1,0:T(8,128)(2,1)S(1)} %stack.10), channel_id=1, replica_groups=mesh['sp'=64,'tp'=4] {'tp'}, dimensions={0} | all-to-all | bytes 16777216 | tf_op jit(solution)/shard_map/all_to_all | solution.py:13
  214.8 4.5 %fusion.2 = f32[2048,512]{1,0:T(8,128)S(1)} fusion(bf16[2048,2048]{1,0:T(8,128)(2,1)S(1)} %bitcast.129, bf16[1,2048,512]{2,1,0:T(8,128)(2,1)S(1)} %copy-done.9), kind=kOutput, calls=%fused_computation.10 | convolution fusion | flops 4294967296 | bytes 14680064 | tf_op jit(solution)/shard_map/erd,edf->erf/dot_general | solution.py:141
  219.3 5.7 %multiply_convert_fusion = bf16[2048,512]{1,0:T(8,128)(2,1)S(1)} fusion(f32[2048,512]{1,0:T(8,128)S(1)} %fusion.2, bf16[2048,2048]{1,0:T(8,128)(2,1)S(1)} %bitcast.130, bf16[1,2048,512]{2,1,0:T(8,128)(2,1)S(1)} %copy-done.10), kind=kOutput, calls=%fused_computation.4 | convolution fusion | flops 4305453056 | bytes 16777216 | tf_op jit(solution)/shard_map/erd,edf->erf/dot_general | solution.py:140
  225.0 6.8 %convert_bitcast_fusion = bf16[1,2048,2048]{2,1,0:T(8,128)(2,1)} fusion(bf16[2048,512]{1,0:T(8,128)(2,1)S(1)} %multiply_convert_fusion, bf16[1,512,2048]{2,1,0:T(8,128)(2,1)S(1)} %copy-done), kind=kOutput, calls=%fused_computation.3 | convolution fusion | flops 4299161600 | bytes 12582912 | tf_op jit(solution)/shard_map/erf,efd->erd/dot_general | solution.py:145
  231.8 0.0 reduce-scatter.2.cloned.1.call-update
  231.8 79.0 %reduce-scatter.2.cloned.1.call-done = bf16[1,512,2048]{2,1,0:T(8,128)(2,1)} async-done(((bf16[1,2048,2048]{2,1,0:T(8,128)(2,1)}), bf16[1,512,2048]{2,1,0:T(8,128)(2,1)}) %reduce-scatter.2.cloned.1.call-update) | async-done | bytes 2097168 | tf_op jit(solution)/shard_map/reduce_scatter | solution.py:146
  310.8 6.7 %copy.103 = bf16[1,512,2048]{2,0,1:T(2,128)(2,1)} copy(bf16[1,512,2048]{2,1,0:T(8,128)(2,1)} %reduce-scatter.2.cloned.1.call-done) | data formatting | bytes 4194304 | tf_op jit(solution)/shard_map/reduce_scatter | solution.py:146
  317.6 0.5 broadcast.379
  318.1 14.7 %reduce.5 = bf16[512,2048]{1,0:T(8,128)(2,1)} reduce(bf16[512,1,2048]{2,1,0:T(2,128)(2,1)} %bitcast.125, bf16[]{:T(256)} %broadcast.379), dimensions={1}, to_apply=%bitcast.122.reduce_sub_computation | reduce | bytes 4194306
  332.8 4.8 %reshape.476 = bf16[64,2,8192]{2,1,0:T(2,128)(2,1)} reshape(bf16[512,2048]{1,0:T(8,128)(2,1)} %reduce.5) | data formatting | bytes 4194304
  337.6 10.9 %all-to-all-start.3 = ((bf16[64,2,8192]{2,1,0:T(2,128)(2,1)}), bf16[64,2,8192]{2,1,0:T(2,128)(2,1)}, u32[]{:S(2)}, u32[]{:S(2)}) async-start(bf16[64,2,8192]{2,1,0:T(2,128)(2,1)} %reshape.476), calls=%async_computation.4 | async-start | bytes 4194304 | tf_op jit(solution)/shard_map/all_to_all | solution.py:147
  348.5 0.1 copy.83
  348.7 51.0 %all-to-all-done.3 = bf16[64,2,8192]{2,1,0:T(2,128)(2,1)} async-done(((bf16[64,2,8192]{2,1,0:T(2,128)(2,1)}), bf16[64,2,8192]{2,1,0:T(2,128)(2,1)}, u32[]{:S(2)}, u32[]{:S(2)}) %all-to-all-start.3) | async-done | bytes 2097184 | tf_op jit(solution)/shard_map/all_to_all | solution.py:147
  399.6 10.4 %reshape.477 = bf16[512,1,2048]{2,1,0:T(2,128)(2,1)} reshape(bf16[64,2,8192]{2,1,0:T(2,128)(2,1)} %all-to-all-done.3) | data formatting | bytes 4194304
  410.1 4.8 %copy.102 = bf16[1,512,2048]{2,1,0:T(8,128)(2,1)} copy(bf16[1,512,2048]{2,0,1:T(2,128)(2,1)} %bitcast.126) | data formatting | bytes 4194304
  414.9 6.9 %gather_fusion.1 = bf16[384,2048]{1,0:T(8,128)(2,1)} fusion(bf16[512,2048]{1,0:T(8,128)(2,1)} %bitcast.124, s32[1024]{0:T(1024)S(1)} %pad_clamp_fusion), kind=kCustom, calls=%fused_computation.1 | custom fusion | bytes 3147264 | tf_op jit(solution)/shard_map/gather | solution.py:148
  421.8 3.6 reshape.437
  425.5 2.4 fusion.47
  427.9 0.3 fusion.13
  428.2 1.2 fusion.16
  (55 shorter events, 0.4 us)
Async XLA Ops:
  6.5 218.5 %copy-start = (bf16[1,512,2048]{2,1,0:T(8,128)(2,1)S(1)}, bf16[1,512,2048]{2,1,0:T(8,128)(2,1)}, u32[]{:S(2)}) copy-start(bf16[1,512,2048]{2,1,0:T(8,128)(2,1)} %param.29) | copy-start | bytes 6291460
  6.5 22.7 %copy-start.3 = (bf16[384,64]{0,1:T(8,128)(2,1)S(1)}, bf16[384,64]{0,1:T(8,128)(2,1)}, u32[]{:S(2)}) copy-start(bf16[384,64]{0,1:T(8,128)(2,1)} %param.18) | copy-start | bytes 147460
  6.5 21.8 %copy-start.5 = (s32[384]{0:T(512)S(1)}, s32[384]{0:T(512)}, u32[]{:S(2)}) copy-start(s32[384]{0:T(512)} %param.19) | copy-start | bytes 4612
  6.5 18.8 %copy-start.11 = (f32[4]{0:T(128)S(1)}, f32[4]{0:T(128)}, u32[]{:S(2)}) copy-start(f32[4]{0:T(128)} %param.20) | copy-start | bytes 52
  8.6 20.7 %collective-permute-start = (bf16[128,128]{0,1:T(8,128)(2,1)S(1)}, bf16[128,128]{0,1:T(8,128)(2,1)S(1)}, u32[]{:S(2)}, u32[]{:S(2)}) collective-permute-start(bf16[128,128]{0,1:T(8,128)(2,1)S(1)} %get-tuple-element.12), channel_id=1, source_target_pairs={{0,4},{4,8},{8,12},{12,16},{16,20},{20,24},{24,28},{28,32},{32,36}... | collective-permute-start | bytes 98312 | tf_op jit(solution)/shard_map/ppermute | solution.py:25
  10.5 18.8 %collective-permute-start.1 = (bf16[128,128]{0,1:T(8,128)(2,1)S(1)}, bf16[128,128]{0,1:T(8,128)(2,1)S(1)}, u32[]{:S(2)}, u32[]{:S(2)}) collective-permute-start(bf16[128,128]{0,1:T(8,128)(2,1)S(1)} %get-tuple-element.13), channel_id=1, source_target_pairs={{4,0},{8,4},{12,8},{16,12},{20,16},{24,20},{28,24},{32,28},{36,32}... | collective-permute-start | bytes 98312 | tf_op jit(solution)/shard_map/ppermute | solution.py:28
  14.9 13.4 %collective-permute-start.2 = (s32[128]{0:T(128)S(1)}, s32[128]{0:T(128)S(1)}, u32[]{:S(2)}, u32[]{:S(2)}) collective-permute-start(s32[128]{0:T(128)S(1)} %get-tuple-element.18), channel_id=1, source_target_pairs={{0,4},{4,8},{8,12},{12,16},{16,20},{20,24},{24,28},{28,32},{32,36}... | collective-permute-start | bytes 1544 | tf_op jit(solution)/shard_map/ppermute | solution.py:25
  16.8 11.5 %collective-permute-start.3 = (s32[128]{0:T(128)S(1)}, s32[128]{0:T(128)S(1)}, u32[]{:S(2)}, u32[]{:S(2)}) collective-permute-start(s32[128]{0:T(128)S(1)} %get-tuple-element.19), channel_id=1, source_target_pairs={{4,0},{8,4},{12,8},{16,12},{20,16},{24,20},{28,24},{32,28},{36,32}... | collective-permute-start | bytes 1544 | tf_op jit(solution)/shard_map/ppermute | solution.py:28
  32.8 10.8 %all-to-all-start = ((bf16[4,96,256]{2,1,0:T(8,128)(2,1)}), bf16[4,96,256]{2,1,0:T(8,128)(2,1)S(1)}, u32[]{:S(2)}, u32[]{:S(2)}) async-start(bf16[4,96,256]{2,1,0:T(8,128)(2,1)} %reshape.471), calls=%async_computation | async-start | bytes 393216 | tf_op jit(solution)/shard_map/all_to_all | solution.py:125
  37.3 273.5 %reduce-scatter.2.cloned.1.call-start = ((), (), s32[]{:S(2)}) async-start(), calls=%async_computation.5 | async-start | bytes 10485760 | tf_op jit(solution)/shard_map/reduce_scatter | solution.py:146
  43.6 3.2 copy-start.1
  43.6 3.2 copy-start.4
  43.7 3.5 copy-start.6
  119.4 95.4 %copy-start.9 = (bf16[1,2048,512]{2,1,0:T(8,128)(2,1)S(1)}, bf16[1,2048,512]{2,1,0:T(8,128)(2,1)}, u32[]{:S(2)}) copy-start(bf16[1,2048,512]{2,1,0:T(8,128)(2,1)} %param.28) | copy-start | bytes 6291460
  214.8 4.5 %copy-start.10 = (bf16[1,2048,512]{2,1,0:T(8,128)(2,1)S(1)}, bf16[1,2048,512]{2,1,0:T(8,128)(2,1)}, u32[]{:S(2)}) copy-start(bf16[1,2048,512]{2,1,0:T(8,128)(2,1)} %param.27) | copy-start | bytes 6291460
  337.6 10.9 %copy-start.8 = (f32[96,4]{0,1:T(4,128)S(1)}, f32[96,4]{0,1:T(4,128)}, u32[]{:S(2)}) copy-start(f32[96,4]{0,1:T(4,128)} %param.26) | copy-start | bytes 4612
  337.6 62.0 %all-to-all-start.3 = ((bf16[64,2,8192]{2,1,0:T(2,128)(2,1)}), bf16[64,2,8192]{2,1,0:T(2,128)(2,1)}, u32[]{:S(2)}, u32[]{:S(2)}) async-start(bf16[64,2,8192]{2,1,0:T(2,128)(2,1)} %reshape.476), calls=%async_computation.4 | async-start | bytes 4194304 | tf_op jit(solution)/shard_map/all_to_all | solution.py:147
  425.5 2.7 copy-start.2
  425.5 2.7 copy-start.7
Sparse Core Ops, SparseCore 0:
  232.0 78.8 reduce-scatter.1
